TPU v7x, 32 devices: a whole 2x2x4 slice. The times are simulated.
32 devices in a mesh: dp: 4 (over y, x), kv: 4 (over z), tp: 2 (over core).
Axes of the slice: x: 2, y: 2, z: 4, core: 2. Of those that a mesh axis runs over, the one named last changes fastest.
Arguments:
- tokens: bfloat16 [32, 4096], P('dp', ('kv', 'tp')), as said below
- query_weight: bfloat16 [4096, 16, 128], P(None, 'tp', 'kv'), may hold values from -0.09375 to 0.09375
- key_weight: bfloat16 [4096, 16, 128], P(None, 'tp', 'kv'), may hold values from -0.09375 to 0.09375
- value_weight: bfloat16 [4096, 16, 256], P(None, 'tp', 'kv'), may hold values from -0.09375 to 0.09375
- gate_weight: bfloat16 [4096, 16, 256], P(None, 'tp', 'kv'), may hold values from -0.09375 to 0.09375
- decay_weight: bfloat16 [4096, 16, 128], P(None, 'tp', 'kv'), may hold values from -0.09375 to 0.09375
- decay_bias: float32 [16, 128], P('tp'), may hold values from -8 to 2
- states: float32 [32, 16, 128, 256], P(('dp', 'kv'), 'tp'), may hold values from -4 to 4
- head_gain: float32 [16, 256], P('tp'), may hold values from 0.1 to 1.9
- out_weight: bfloat16 [4096, 4096], P(None, ('kv', 'tp')), as said below
- norm1_gain: float32 [4096], P(('kv', 'tp')), may hold values from 0.1 to 1.9
- norm1_bias: float32 [4096], P(('kv', 'tp')), may hold values from -3 to 3
- up_weight: bfloat16 [4096, 16384], P(None, ('kv', 'tp')), may hold values from -0.09375 to 0.09375
- down_weight: bfloat16 [16384, 4096], P(('kv', 'tp')), as said below
- norm2_gain: float32 [4096], P(('kv', 'tp')), may hold values from 0.1 to 1.9
- norm2_bias: float32 [4096], P(('kv', 'tp')), may hold values from -3 to 3
Outputs:
- layer_out: bfloat16 [32, 4096], P('dp', ('kv', 'tp'))
- new_states: float32 [32, 16, 128, 256], P(('dp', 'kv'), 'tp')
Inputs may be any that keep to these rules, and one draw needn't show every extreme that they name: `tokens`: each block of 64 features has its own scale. `out_weight`: entries lie within 13 / sqrt(4096) of zero. `down_weight`: entries lie within 14 / sqrt(16384) of zero.
All inputs are finite; a program needn't handle non-finite values.
Results may differ from a plain program's by a relative error of at most 0.009.
Values may be sent and summed in bfloat16 or wider, within the bound.
A program may use at most 128 MiB of HBM per device.

v0:
```python
import jax
import jax.numpy as jnp
from jax import lax
from jax.sharding import PartitionSpec as P

D = 4096
KEY_DIM = 128


ALPHA = 2.0**0.5
TAU = 16.0
LN_EPS = 1e-05
RMS_EPS = 1e-06


def project_flat(inputs, weight):
    flattened = weight.reshape(weight.shape[0], -1)
    return jnp.dot(inputs, flattened, preferred_element_type=jnp.float32).astype(jnp.bfloat16)


def normalize(inputs, average, spread, row_gain, row_shift):
    return ((inputs - average) * lax.rsqrt(spread + LN_EPS) * row_gain + row_shift).astype(
        jnp.bfloat16
    )


def body(
    tokens,
    query_weight,
    key_weight,
    value_weight,
    gate_weight,
    decay_weight,
    decay_bias,
    states,
    head_gain,
    out_weight,
    norm1_gain,
    norm1_bias,
    up_weight,
    down_weight,
    norm2_gain,
    norm2_bias,
):
    whole = lax.all_gather(tokens, ("kv", "tp"), axis=1, tiled=True)
    weights_list = (query_weight, key_weight, decay_weight, value_weight, gate_weight)
    packed = jnp.concatenate([project_flat(whole, weight) for weight in weights_list], axis=1)
    arrived = lax.all_to_all(packed, "kv", split_axis=0, concat_axis=0, tiled=True)
    groups = lax.axis_size("kv")
    seq_count = whole.shape[0] // groups
    local_heads = query_weight.shape[1]
    unpacked = []
    start = 0
    for weight in weights_list:
        channels = weight.shape[2]
        width = local_heads * channels
        block = arrived[:, start : start + width].reshape(groups, seq_count, local_heads, channels)
        block = block.transpose(1, 2, 0, 3).reshape(seq_count, local_heads, groups * channels)
        unpacked.append(block.astype(jnp.float32))
        start = start + width
    query_rows = unpacked[0] * KEY_DIM ** (-0.5)
    key_rows = unpacked[1]
    decay_rows = unpacked[2]
    value_rows = unpacked[3]
    gate_rows = unpacked[4]
    retain = jnp.exp(jax.nn.log_sigmoid(decay_rows + decay_bias) / TAU)
    new_states = retain[..., None] * states + key_rows[..., :, None] * value_rows[..., None, :]
    readout = jnp.einsum("shk,shkv->shv", query_rows, new_states, precision=lax.Precision.HIGHEST)
    readout = (
        readout
        * lax.rsqrt(jnp.mean(readout * readout, axis=-1, keepdims=True) + RMS_EPS)
        * head_gain
    )
    attended = (readout * jax.nn.silu(gate_rows)).astype(jnp.bfloat16)
    seq_count, local_heads, value_width = attended.shape
    flat_width = local_heads * value_width
    collected = lax.all_gather(
        attended.reshape(1, seq_count, flat_width), ("kv", "tp"), axis=0, tiled=True
    )
    halves = lax.axis_size("tp")
    collected = collected.reshape(-1, halves, seq_count, flat_width)
    columns = out_weight.shape[1]
    out_parts = out_weight.reshape(halves, flat_width, columns)
    mixed_heads = jnp.einsum(
        "atsc,tcd->asd", collected, out_parts, preferred_element_type=jnp.float32
    ).reshape(-1, columns)
    residual_one = ALPHA * tokens.astype(jnp.float32) + mixed_heads
    offset = lax.axis_index(("kv", "tp")) * columns
    totals = lax.psum(
        (
            jnp.sum(residual_one, axis=-1, keepdims=True),
            jnp.sum(residual_one * residual_one, axis=-1, keepdims=True),
        ),
        ("kv", "tp"),
    )
    average = totals[0] / D
    spread = totals[1] / D - average * average
    normed_own = normalize(residual_one, average, spread, norm1_gain, norm1_bias)
    normed = lax.all_gather(normed_own, ("kv", "tp"), axis=1, tiled=True)
    lifted = jnp.dot(normed, up_weight, preferred_element_type=jnp.float32)
    hidden = jnp.square(jax.nn.relu(lifted)).astype(jnp.bfloat16)
    mixer_term = jnp.dot(hidden, down_weight, preferred_element_type=jnp.float32)
    mixer_all = lax.psum(mixer_term, ("kv", "tp"))
    residual_two = ALPHA * normed.astype(jnp.float32) + mixer_all
    average = jnp.sum(residual_two, axis=-1, keepdims=True) / D
    spread = jnp.sum(residual_two * residual_two, axis=-1, keepdims=True) / D - average * average
    own_rows = lax.dynamic_slice_in_dim(residual_two, offset, columns, 1)
    layer_out = normalize(own_rows, average, spread, norm2_gain, norm2_bias)
    return (layer_out, new_states)


def solution(mesh):
    placed = (
        P("dp", ("kv", "tp")),
        P(None, "tp", "kv"),
        P(None, "tp", "kv"),
        P(None, "tp", "kv"),
        P(None, "tp", "kv"),
        P(None, "tp", "kv"),
        P("tp", None),
        P(("dp", "kv"), "tp", None, None),
        P("tp", None),
        P(None, ("kv", "tp")),
        P(("kv", "tp")),
        P(("kv", "tp")),
        P(None, ("kv", "tp")),
        P(("kv", "tp"), None),
        P(("kv", "tp")),
        P(("kv", "tp")),
    )
    return jax.shard_map(
        body,
        mesh=mesh,
        in_specs=placed,
        out_specs=(P("dp", ("kv", "tp")), P(("dp", "kv"), "tp", None, None)),
        check_vma=False,
    )
```

profile of v0, /device:TPU:0, one launch (start us, length us, event | category | flops | bytes accessed | tf_op | source)
XLA Modules:
  0.0 167.2 jit_solution(12161936013294554536)
XLA Ops:
  7.2 0.0 copy-start
  7.2 0.0 all-reduce.3.cloned.1.call-start
  7.2 0.0 copy-start.4
  7.2 16.0 %all_gather.9 = bf16[8,4096]{1,0:T(8,128)(2,1)S(1)} all-gather(bf16[8,512]{1,0:T(8,128)(2,1)} %param.16), channel_id=1, replica_groups=mesh['dp'=4,'kv'=4,'tp'=2] {'kv','tp'}, dimensions={1}, use_global_device_ids=true | all-gather | bytes 73728 | tf_op jit(solution)/shard_map/all_gather | solution.py:45
  23.3 0.0 copy-done
  23.3 0.6 fusion.7
  23.9 0.0 copy-done.4
  23.9 0.0 copy-start.2
  23.9 0.7 fusion.6
  24.6 2.6 %fusion.5 = bf16[8,1792]{1,0:T(8,128)(2,1)S(1)} fusion(bf16[8,1792]{1,0:T(8,128)(2,1)S(1)} %fusion.6, bf16[8,4096]{1,0:T(8,128)(2,1)S(1)} %all_gather.9, bf16[4096,256]{0,1:T(8,128)(2,1)} %bitcast.60), kind=kOutput, calls=%fused_computation.11 | convolution fusion | flops 16779264 | bytes 2166784 | tf_op jit(solution)/shard_map/dot_general | solution.py:18
  27.2 0.0 copy-done.2
  27.2 0.0 copy-start.3
  27.2 1.2 fusion.4
  28.4 1.0 copy-done.3
  29.4 0.0 copy-start.7
  29.4 1.2 fusion.3
  30.6 10.1 %all_to_all.12 = bf16[4,2,1792]{2,1,0:T(2,128)(2,1)S(1)} all-to-all(bf16[4,2,1792]{2,1,0:T(2,128)(2,1)S(1)} %all_to_all.8), channel_id=1, replica_groups=mesh['dp'=4,'kv'=4,'tp'=2] {'kv'}, dimensions={0} | all-to-all | bytes 57344 | tf_op jit(solution)/shard_map/all_to_all | solution.py:48
  40.7 0.1 reshape.138
  40.8 0.1 reshape.134
  40.9 0.1 reshape.136
  41.0 0.1 reshape.132
  41.1 0.1 reshape.137
  41.2 0.1 reshape.133
  41.3 0.1 mul.135
  41.4 0.1 reshape.140
  41.4 0.0 copy-done.7
  41.5 1.9 %multiply_add_fusion = f32[2,8,128,256]{3,2,1,0:T(8,128)S(1)} fusion(f32[2,8,128,256]{3,2,1,0:T(8,128)} %param.23, f32[2,8,256]{2,1,0:T(8,128)S(1)} %reshape.134, f32[2,8,128]{2,1,0:T(8,128)S(1)} %reshape.133, f32[2,8,128]{2,1,0:T(8,128)S(1)} %fusion.16), kind=kLoop, calls=%fused_computation.3 | loop fusion | flops 1572864 | bytes 4227072 | tf_op jit(solution)/shard_map/add | solution.py:67
  43.4 0.0 copy-start.1
  43.4 0.0 copy-start.6
  43.4 0.0 copy-start.5
  43.4 1.3 copy-done.1
  44.7 1.1 fusion.20
  45.8 0.1 fusion.10
  45.9 0.1 reshape.139
  46.0 0.1 reshape.135
  46.1 0.0 copy-done.6
  46.1 0.1 fusion.13
  46.2 14.0 %all_gather.10 = bf16[8,2,2048]{2,1,0:T(2,128)(2,1)S(1)} all-gather(bf16[1,2,2048]{2,1,0:T(2,128)(2,1)S(1)} %reshape.129), channel_id=1, replica_groups=mesh['dp'=4,'kv'=4,'tp'=2] {'kv','tp'}, dimensions={0}, use_global_device_ids=true | all-gather | bytes 73728 | tf_op jit(solution)/shard_map/all_gather | solution.py:77
  60.3 0.0 copy-done.5
  60.3 0.0 copy-start.8
  60.3 0.0 copy-start.9
  60.3 3.0 %fusion.19 = (f32[8]{0:T(128)S(1)}, f32[8]{0:T(128)S(1)}, f32[8,512]{1,0:T(8,128)S(1)}) fusion(bf16[8,2048,2]{1,0,2:T(8,128)(2,1)S(1)} %dot_general.38, bf16[2,2048,512]{2,1,0:T(8,128)(2,1)} %bitcast.56, bf16[8,512]{1,0:T(8,128)(2,1)S(1)} %copy-done.5), kind=kOutput, calls=%fused_computation.45 | convolution fusion | flops 33578992 | bytes 4284480 | tf_op jit(solution)/shard_map/atsc,tcd->asd/dot_general | solution.py:84
  63.3 14.2 %all-reduce = (f32[8,1]{0,1:T(1,128)S(1)}, f32[8,1]{0,1:T(1,128)S(1)}) all-reduce(f32[8,1]{0,1:T(1,128)S(1)} %bitcast.69, f32[8,1]{0,1:T(1,128)S(1)} %bitcast.68), channel_id=1, replica_groups=mesh['dp'=4,'kv'=4,'tp'=2] {'kv','tp'}, use_global_device_ids=true, to_apply=%region_4.5 | all-reduce | flops 16 | bytes 128 | tf_op jit(solution)/shard_map/psum | solution.py:89
  77.6 0.0 copy-done.8
  77.6 0.0 copy-done.9
  77.6 0.1 add_convert_fusion.1
  77.7 14.0 %all_gather.11 = bf16[8,4096]{1,0:T(8,128)(2,1)S(1)} all-gather(bf16[8,512]{1,0:T(8,128)(2,1)S(1)} %add_convert_fusion.1), channel_id=1, replica_groups=mesh['dp'=4,'kv'=4,'tp'=2] {'kv','tp'}, dimensions={1}, use_global_device_ids=true | all-gather | bytes 73728 | tf_op jit(solution)/shard_map/all_gather | solution.py:99
  91.6 0.0 copy-start.10
  91.6 0.0 copy-start.11
  91.6 13.5 %fusion.8 = f32[8,4096]{1,0:T(8,128)} fusion(bf16[2048,4096]{1,0:T(8,128)(2,1)} %param.29, bf16[8,4096]{1,0:T(8,128)(2,1)S(1)} %all_gather.11, bf16[4096,2048]{1,0:T(8,128)(2,1)} %param.28), kind=kOutput, calls=%fused_computation.16 | convolution fusion | flops 268484608 | bytes 33751040 | tf_op jit(solution)/shard_map/dot_general | solution.py:102
  105.2 0.0 all-reduce.3.cloned.1.call-update
  105.2 53.4 %all-reduce.3.cloned.1.call-done = f32[8,4096]{1,0:T(8,128)} async-done(((f32[8,4096]{1,0:T(8,128)}), f32[8,4096]{1,0:T(8,128)}) %all-reduce.3.cloned.1.call-update) | async-done | bytes 131088 | tf_op jit(solution)/shard_map/psum | solution.py:103
  158.5 1.1 fusion.18
  159.6 0.0 copy-done.10
  159.6 0.0 copy-done.11
  159.6 0.7 add_convert_fusion
  (17 shorter events, 0.3 us)
Async XLA Ops:
  7.2 16.1 %copy-start = (bf16[4096,8,32]{0,2,1:T(8,128)(2,1)S(1)}, bf16[4096,8,32]{0,2,1:T(8,128)(2,1)}, u32[]{:S(2)}) copy-start(bf16[4096,8,32]{0,2,1:T(8,128)(2,1)} %param.17) | copy-start | bytes 6291460
  7.2 151.4 %all-reduce.3.cloned.1.call-start = ((), (), s32[]{:S(2)}) async-start(), calls=%async_computation.1 | async-start | bytes 262144 | tf_op jit(solution)/shard_map/psum | solution.py:103
  7.2 16.7 %copy-start.4 = (bf16[4096,8,32]{0,2,1:T(8,128)(2,1)S(1)}, bf16[4096,8,32]{0,2,1:T(8,128)(2,1)}, u32[]{:S(2)}) copy-start(bf16[4096,8,32]{0,2,1:T(8,128)(2,1)} %param.18) | copy-start | bytes 6291460
  23.9 3.2 %copy-start.2 = (bf16[4096,8,64]{0,2,1:T(8,128)(2,1)S(1)}, bf16[4096,8,64]{0,2,1:T(8,128)(2,1)}, u32[]{:S(2)}) copy-start(bf16[4096,8,64]{0,2,1:T(8,128)(2,1)} %param.19) | copy-start | bytes 12582916
  27.2 2.2 %copy-start.3 = (bf16[4096,8,64]{0,2,1:T(8,128)(2,1)S(1)}, bf16[4096,8,64]{0,2,1:T(8,128)(2,1)}, u32[]{:S(2)}) copy-start(bf16[4096,8,64]{0,2,1:T(8,128)(2,1)} %param.20) | copy-start | bytes 12582916
  29.4 12.1 %copy-start.7 = (f32[8,128]{1,0:T(8,128)S(1)}, f32[8,128]{1,0:T(8,128)}, u32[]{:S(2)}) copy-start(f32[8,128]{1,0:T(8,128)} %param.22) | copy-start | bytes 12292
  43.4 1.3 copy-start.1
  43.4 2.7 %copy-start.6 = (f32[8,256]{1,0:T(8,128)S(1)}, f32[8,256]{1,0:T(8,128)}, u32[]{:S(2)}) copy-start(f32[8,256]{1,0:T(8,128)} %param.24) | copy-start | bytes 24580
  43.4 16.9 %copy-start.5 = (bf16[8,512]{1,0:T(8,128)(2,1)S(1)}, bf16[8,512]{1,0:T(8,128)(2,1)}, u32[]{:S(2)}) copy-start(bf16[8,512]{1,0:T(8,128)(2,1)} %param.16) | copy-start | bytes 24580
  60.3 17.3 %copy-start.8 = (f32[512]{0:T(512)S(1)}, f32[512]{0:T(512)}, u32[]{:S(2)}) copy-start(f32[512]{0:T(512)} %param.27) | copy-start | bytes 6148
  60.3 17.3 %copy-start.9 = (f32[512]{0:T(512)S(1)}, f32[512]{0:T(512)}, u32[]{:S(2)}) copy-start(f32[512]{0:T(512)} %param.26) | copy-start | bytes 6148
  91.6 68.0 %copy-start.10 = (f32[512]{0:T(512)S(1)}, f32[512]{0:T(512)}, u32[]{:S(2)}) copy-start(f32[512]{0:T(512)} %param.31) | copy-start | bytes 6148
  91.6 68.0 %copy-start.11 = (f32[512]{0:T(512)S(1)}, f32[512]{0:T(512)}, u32[]{:S(2)}) copy-start(f32[512]{0:T(512)} %param.30) | copy-start | bytes 6148
Sparse Core Ops, SparseCore 0:
  105.3 53.1 all-reduce.2
where the time goes:
time: 167 us
  blocking collectives  68.3 us (41%)
  waiting for transfers between devices  53.4 us (32%)
  matrix products  23.9 us (14%)
  between operations  14.2 us (9%)
  other arithmetic  4 us (2%)
  local copies, waits for them, and re-layouts  3.36 us (2%)
    psum x1, waiting for transfers between devices, body(): mixer_all = lax.psum(mixer_term, ('kv', 'tp'))  53.4 us
    all_gather x1, blocking collectives, body(): whole = lax.all_gather(tokens, ('kv', 'tp'), axis=1, tiled=True)  16 us
    psum x1, blocking collectives, body(): lax.psum((jnp.sum(residual_one, axis=-1, keepdims=True), jnp.sum(residual...  14.2 us
    all_gather x1, blocking collectives, body(): lax.all_gather(attended.reshape(1, seq_count, flat_width), ('kv', 'tp'),...  14 us
    all_gather x1, blocking collectives, body(): normed = lax.all_gather(normed_own, ('kv', 'tp'), axis=1, tiled=True)  14 us
    dot_general x1, matrix products, body(): jnp.dot(hidden, down_weight, preferred_element_type=jnp.float32)  13.5 us
    all_to_all x1, blocking collectives, body(): lax.all_to_all(packed, 'kv', split_axis=0, concat_axis=0, tiled=True)  10.1 us
    dot_general x5, matrix products, project_flat(): jnp.dot(inputs, flattened, preferred_element_type=jnp.float32)  6.25 us
  transfers between devices with their start and end apart: 1, of which 1 were waited for; matrix products, arithmetic and copies ran while one was open for 0% of the time, Pallas kernels for 0%

commit v1 on v0

--- a/solution.py
+++ b/solution.py
@@ -1,6 +1,10 @@
+import functools
+
 import jax
 import jax.numpy as jnp
 from jax import lax
+from jax.experimental import pallas as pl
+from jax.experimental.pallas import tpu as pltpu
 from jax.sharding import PartitionSpec as P
 
 D = 4096
@@ -109,6 +113,335 @@
     return (layer_out, new_states)
 
 
+MESH = pl.DeviceIdType.MESH
+F32 = jnp.float32
+BF16 = jnp.bfloat16
+
+
+def dot_nt(left, right):
+    return lax.dot_general(left, right, (((1,), (1,)), ((), ())), preferred_element_type=F32)
+
+
+def layer_kernel(
+    groups, halves, tokens, wq, wk, wd, wv, wg, bias, states, head_gain, wout, gain1, shift1,
+    wup, wdown, gain2, shift2,
+    out, states_out,
+    tok_v, proj_v, out_v, up_v, down_v, state_v, bias_v, hgain_v, gain1_v, shift1_v, gain2_v,
+    shift2_v, own_g1, own_s1, bias_t, x_v, a_send, a_recv, a_rows, att_rows, gate_rows, att_recv,
+    x_rows, r_own, r_all, normed_v, hidden_v, p_send, p_recv, s_send, s_recv, res_v,
+    load_sem, x_ss, x_rs, a_ss, a_rs, t_ss, t_rs, r_ss, r_rs, p_ss, p_rs, s_ss, s_rs, g_ss, g_rs,
+    b_ss, b_rs,
+):
+    members = groups * halves
+    my_kv, my_tp = lax.axis_index("kv"), lax.axis_index("tp")
+    me = my_kv * halves + my_tp
+    rows, cols = tok_v.shape
+    width = x_v.shape[1]
+    seqs = rows // groups
+    heads, kdim = bias_v.shape
+    vdim = hgain_v.shape[1]
+    kc, vc = kdim // groups, vdim // groups
+    nk, nv = heads * kc, heads * vc
+
+    def load(index, src, dst):
+        copy = pltpu.make_async_copy(src, dst, load_sem.at[index])
+        copy.start()
+        return copy
+
+    loads = {}
+    loads["tok"] = load(0, tokens, tok_v)
+    loads["g1"] = load(1, gain1, own_g1)
+    loads["s1"] = load(2, shift1, own_s1)
+    loads["bias"] = load(3, bias, bias_v)
+    start = 0
+    for index, (name, weight) in enumerate((("q", wq), ("k", wk), ("d", wd), ("v", wv), ("g", wg))):
+        size = weight.shape[0]
+        loads[name] = load(4 + index, weight, proj_v.at[pl.ds(start, size)])
+        start += size
+    loads["hg"] = load(9, head_gain, hgain_v)
+    loads["g2"] = load(10, gain2, gain2_v)
+    loads["s2"] = load(11, shift2, shift2_v)
+    loads["st"] = load(12, states, state_v)
+    loads["out"] = load(13, wout, out_v)
+    loads["up"] = load(14, wup, up_v)
+    loads["down"] = load(15, wdown, down_v)
+
+    def member(offset):
+        index = lax.rem(me + offset, members)
+        return index, {"kv": index // halves, "tp": lax.rem(index, halves)}
+
+    def block(index):
+        return pl.ds(pl.multiple_of(index * cols, cols), cols)
+
+    barrier = pltpu.get_barrier_semaphore()
+    for o in range(1, members):
+        pl.semaphore_signal(barrier, inc=1, device_id=member(o)[1], device_id_type=MESH)
+    pl.semaphore_wait(barrier, members - 1)
+
+    def remote(src, dst, send, recv, target):
+        return pltpu.make_async_remote_copy(
+            src_ref=src, dst_ref=dst, send_sem=send, recv_sem=recv, device_id=target,
+            device_id_type=MESH,
+        )
+
+    def spread(src, place, send, recv):
+        copies = []
+        for o in range(1, members):
+            copy = remote(src, place(me), send.at[o], recv.at[o], member(o)[1])
+            copy.start()
+            copies.append(copy)
+        return copies
+
+    def collect(src, place, send, recv):
+        for o in range(1, members):
+            source, target = member(members - o)
+            remote(src, place(source), send.at[o], recv.at[o], target).wait_recv()
+
+    pending = []
+    loads["tok"].wait()
+    pending += spread(tok_v, lambda i: x_v.at[:, block(i)], x_ss, x_rs)
+    x_v[:, block(me)] = tok_v[...]
+    loads["g1"].wait()
+    loads["s1"].wait()
+    pending += spread(own_g1, lambda i: gain1_v.at[:, block(i)], g_ss, g_rs)
+    pending += spread(own_s1, lambda i: shift1_v.at[:, block(i)], b_ss, b_rs)
+    gain1_v[:, block(me)] = own_g1[...]
+    shift1_v[:, block(me)] = own_s1[...]
+
+    loads["bias"].wait()
+    turned = jnp.concatenate([bias_v[...], jnp.zeros((kdim - heads, kdim), F32)], axis=0).T
+    lane = lax.broadcasted_iota(jnp.int32, (kc, rows), 1)
+    for h in range(heads):
+        piece = jnp.zeros((kc, rows), F32)
+        for b in range(groups):
+            here = (lane >= b * seqs) & (lane < (b + 1) * seqs)
+            piece = jnp.where(here, turned[b * kc : (b + 1) * kc, h : h + 1], piece)
+        bias_t[h * kc : (h + 1) * kc, :] = piece
+
+    collect(tok_v, lambda i: x_v.at[:, block(i)], x_ss, x_rs)
+    x_all = x_v[...]
+
+    def store_projection(first, size):
+        got = dot_nt(x_all, proj_v[first : first + size, :]).astype(BF16).astype(F32)
+        for a in range(groups):
+            a_send[a, :, first : first + size] = got[a * seqs : (a + 1) * seqs, :]
+
+    loads["q"].wait()
+    loads["k"].wait()
+    store_projection(0, 2 * nk)
+    loads["d"].wait()
+    store_projection(2 * nk, nk)
+    loads["v"].wait()
+    store_projection(3 * nk, nv)
+    loads["g"].wait()
+    store_projection(3 * nk + nv, nv)
+
+    for o in range(1, groups):
+        peer = lax.rem(my_kv + o, groups)
+        copy = remote(
+            a_send.at[peer], a_recv.at[my_kv], a_ss.at[o], a_rs.at[o], {"kv": peer, "tp": my_tp}
+        )
+        copy.start()
+        pending.append(copy)
+    a_recv[my_kv] = a_send[my_kv]
+    for o in range(1, groups):
+        peer = lax.rem(my_kv + groups - o, groups)
+        remote(
+            a_send.at[peer], a_recv.at[peer], a_ss.at[o], a_rs.at[o], {"kv": peer, "tp": my_tp}
+        ).wait_recv()
+    for b in range(groups):
+        a_rows[b * seqs : (b + 1) * seqs, :] = a_recv[b]
+
+    qt = a_rows[:, 0:nk].T * KEY_DIM ** (-0.5)
+    kt = a_rows[:, nk : 2 * nk].T
+    zt = a_rows[:, 2 * nk : 3 * nk].T + bias_t[...]
+    rt = jnp.exp((jnp.minimum(zt, 0.0) - jnp.log1p(jnp.exp(-jnp.abs(zt)))) / TAU)
+    loads["st"].wait()
+    for s in range(seqs):
+        for h in range(heads):
+            first = 3 * nk + h * vc
+            values, gates = [], []
+            for b in range(groups):
+                row = b * seqs + s
+                values.append(a_rows[row : row + 1, first : first + vc])
+                gates.append(a_rows[row : row + 1, first + nv : first + nv + vc])
+            value = jnp.concatenate(values, axis=1)
+            gate_rows[s : s + 1, h * vdim : (h + 1) * vdim] = jnp.concatenate(gates, axis=1)
+            total = None
+            for b in range(groups):
+                lanes = slice(b * seqs + s, b * seqs + s + 1)
+                subs = slice(h * kc, (h + 1) * kc)
+                fresh = (
+                    rt[subs, lanes] * state_v[s, h, b * kc : (b + 1) * kc, :]
+                    + kt[subs, lanes] * value
+                )
+                state_v[s, h, b * kc : (b + 1) * kc, :] = fresh
+                term = qt[subs, lanes] * fresh
+                total = term if total is None else total + term
+            att_rows[s : s + 1, h * vdim : (h + 1) * vdim] = jnp.sum(total, axis=0, keepdims=True)
+    loads["hg"].wait()
+    for h in range(heads):
+        span = slice(h * vdim, (h + 1) * vdim)
+        readout = att_rows[:, span]
+        gate = gate_rows[:, span]
+        power = jnp.mean(readout * readout, axis=-1, keepdims=True)
+        readout = readout * lax.rsqrt(power + RMS_EPS) * hgain_v[h : h + 1, :]
+        att_rows[:, span] = (readout * (gate / (1.0 + jnp.exp(-gate)))).astype(BF16).astype(F32)
+
+    pending += spread(att_rows, lambda i: att_recv.at[i], t_ss, t_rs)
+    save = pltpu.make_async_copy(state_v, states_out, load_sem.at[16])
+    save.start()
+    att_recv[me] = att_rows[...]
+    collect(att_rows, lambda i: att_recv.at[i], t_ss, t_rs)
+    half = heads * vdim
+    for a in range(groups):
+        for t in range(halves):
+            x_rows[a * seqs : (a + 1) * seqs, t * half : (t + 1) * half] = att_recv[a * halves + t]
+    loads["out"].wait()
+    mixed = jnp.dot(x_rows[...].astype(BF16), out_v[...], preferred_element_type=F32)
+    r_own[...] = ALPHA * tok_v[...].astype(F32) + mixed
+    pending += spread(r_own, lambda i: r_all.at[:, block(i)], r_ss, r_rs)
+    r_all[:, block(me)] = r_own[...]
+    collect(own_g1, lambda i: gain1_v.at[:, block(i)], g_ss, g_rs)
+    collect(own_s1, lambda i: shift1_v.at[:, block(i)], b_ss, b_rs)
+    collect(r_own, lambda i: r_all.at[:, block(i)], r_ss, r_rs)
+    whole = r_all[...]
+    average = jnp.sum(whole, axis=-1, keepdims=True) / width
+    spread_one = jnp.sum(whole * whole, axis=-1, keepdims=True) / width - average * average
+    normed = normalize(whole, average, spread_one, gain1_v[...], shift1_v[...])
+    normed_v[...] = normed
+
+    loads["up"].wait()
+    units = up_v.shape[1]
+    step = min(units, 512)
+
+    def lift(i, carry):
+        span = pl.ds(pl.multiple_of(i * step, step), step)
+        lifted = jnp.dot(normed_v[...], up_v[:, span], preferred_element_type=F32)
+        hidden_v[:, span] = jnp.square(jnp.maximum(lifted, 0.0)).astype(BF16)
+        return carry
+
+    lax.fori_loop(0, units // step, lift, 0)
+    loads["down"].wait()
+
+    def drop(o, carry):
+        index, target = member(o)
+        p_send[o] = jnp.dot(hidden_v[...], down_v[:, block(index)], preferred_element_type=F32)
+        remote(p_send.at[o], p_recv.at[o], p_ss.at[o], p_rs.at[o], target).start()
+        return carry
+
+    lax.fori_loop(1, members, drop, 0)
+    total = jnp.dot(hidden_v[...], down_v[:, block(me)], preferred_element_type=F32)
+    total = total + ALPHA * normed_v[:, block(me)].astype(F32)
+    for o in range(1, members):
+        target = member(members - o)[1]
+        remote(p_send.at[o], p_recv.at[o], p_ss.at[o], p_rs.at[o], target).wait_recv()
+        total = total + p_recv[o]
+    sums = jnp.sum(total, axis=-1, keepdims=True)
+    squares = jnp.sum(total * total, axis=-1, keepdims=True)
+    lane = lax.broadcasted_iota(jnp.int32, s_send.shape, 1)
+    stats = jnp.where(lane == 0, sums, squares)
+    s_send[...] = stats
+    pending += spread(s_send, lambda i: s_recv.at[i], s_ss, s_rs)
+    loads["g2"].wait()
+    loads["s2"].wait()
+    for o in range(1, members):
+        source, target = member(members - o)
+        remote(s_send, s_recv.at[source], s_ss.at[o], s_rs.at[o], target).wait_recv()
+        stats = stats + s_recv[source]
+    average = stats[:, 0:1] / width
+    spread_two = stats[:, 1:2] / width - average * average
+    res_v[...] = normalize(total, average, spread_two, gain2_v[...], shift2_v[...])
+    result = pltpu.make_async_copy(res_v, out, load_sem.at[17])
+    result.start()
+    for copy in pending:
+        copy.wait_send()
+    for o in range(1, members):
+        remote(p_send.at[o], p_recv.at[o], p_ss.at[o], p_rs.at[o], member(o)[1]).wait_send()
+    save.wait()
+    result.wait()
+
+
+def fused(groups, halves, *arrays):
+    (tokens, wq, wk, wv, wg, wd, bias, states, head_gain, wout, gain1, shift1, wup, wdown, gain2,
+     shift2) = arrays
+
+    def flat(weight):
+        return weight.transpose(1, 2, 0).reshape(-1, weight.shape[0])
+
+    def row(vector):
+        return vector.reshape(1, -1)
+
+    rows, cols = tokens.shape
+    members = groups * halves
+    width = wq.shape[0]
+    seqs, heads, kdim, vdim = states.shape
+    proj = 3 * wq.shape[1] * wq.shape[2] + 2 * wv.shape[1] * wv.shape[2]
+    vmem = pltpu.VMEM
+    dma = pltpu.SemaphoreType.DMA
+    anywhere = pl.BlockSpec(memory_space=pl.ANY)
+    scratch = [
+        vmem((rows, cols), BF16),
+        vmem((proj, width), BF16),
+        vmem(wout.shape, BF16),
+        vmem(wup.shape, BF16),
+        vmem(wdown.shape, BF16),
+        vmem(states.shape, F32),
+        vmem(bias.shape, F32),
+        vmem(head_gain.shape, F32),
+        vmem((1, width), F32),
+        vmem((1, width), F32),
+        vmem((1, cols), F32),
+        vmem((1, cols), F32),
+        vmem((1, cols), F32),
+        vmem((1, cols), F32),
+        vmem((heads * kdim // groups, rows), F32),
+        vmem((rows, width), BF16),
+        vmem((groups, seqs, proj), F32),
+        vmem((groups, seqs, proj), F32),
+        vmem((rows, proj), F32),
+        vmem((seqs, heads * vdim), F32),
+        vmem((seqs, heads * vdim), F32),
+        vmem((members, seqs, heads * vdim), F32),
+        vmem((rows, halves * heads * vdim), F32),
+        vmem((rows, cols), F32),
+        vmem((rows, width), F32),
+        vmem((rows, width), BF16),
+        vmem((rows, wup.shape[1]), BF16),
+        vmem((members, rows, cols), F32),
+        vmem((members, rows, cols), F32),
+        vmem((rows, 128), F32),
+        vmem((members, rows, 128), F32),
+        vmem((rows, cols), BF16),
+        dma((18,)),
+    ]
+    for count in (members, groups, members, members, members, members, members, members):
+        scratch += [dma((count,)), dma((count,))]
+    return pl.pallas_call(
+        functools.partial(layer_kernel, groups, halves),
+        out_shape=(
+            jax.ShapeDtypeStruct(tokens.shape, BF16),
+            jax.ShapeDtypeStruct(states.shape, F32),
+        ),
+        in_specs=[anywhere] * 16,
+        out_specs=(anywhere, anywhere),
+        scratch_shapes=scratch,
+        compiler_params=pltpu.CompilerParams(
+            collective_id=0, has_side_effects=True, vmem_limit_bytes=67043328
+        ),
+    )(
+        tokens, flat(wq), flat(wk), flat(wd), flat(wv), flat(wg), bias, states, head_gain, wout,
+        row(gain1), row(shift1), wup, wdown, row(gain2), row(shift2),
+    )
+
+
+def dispatch(groups, halves, *arrays):
+    rows, cols = arrays[0].shape
+    if rows == 8 and cols % 128 == 0 and rows % groups == 0:
+        return fused(groups, halves, *arrays)
+    return body(*arrays)
+
+
 def solution(mesh):
     placed = (
         P("dp", ("kv", "tp")),
@@ -129,7 +462,7 @@
         P(("kv", "tp")),
     )
     return jax.shard_map(
-        body,
+        functools.partial(dispatch, mesh.shape["kv"], mesh.shape["tp"]),
         mesh=mesh,
         in_specs=placed,
         out_specs=(P("dp", ("kv", "tp")), P(("dp", "kv"), "tp", None, None)),

time: 167 us -> 48.1 us (0.29)
  blocking collectives: 68.3 us -> 0 us
  waiting for transfers between devices: 53.4 us -> 0 us
  Pallas kernels: 0 us -> 42.9 us
  matrix products: 23.9 us -> 0 us
  between operations: 14.2 us -> 0.65 us
  other arithmetic: 4 us -> 0 us
    psum x1 -> x0, waiting for transfers between devices: 53.4 us -> none  [body(): mixer_all = lax.psum(mixer_term, ('kv', 'tp'))]
    all_gather x3 -> x0, blocking collectives: 44 us -> none  [the longest x1 16 us: body(): whole = lax.all_gather(tokens, ('kv', 'tp'), axis=1, tiled=True)]
    pallas_call x0 -> x1, Pallas kernels: none -> 42.9 us  [fused(): pl.pallas_call(functools.partial(layer_kernel, groups, halves), out_shape...]
    dot_general x8 -> x0, matrix products: 23.9 us -> none  [the longest x1 13.5 us: body(): jnp.dot(hidden, down_weight, preferred_element_type=jnp.float32)]
    psum x1 -> x0, blocking collectives: 14.2 us -> none  [body(): lax.psum((jnp.sum(residual_one, axis=-1, keepdims=True), jnp.sum(residual...]
    all_to_all x1 -> x0, blocking collectives: 10.1 us -> none  [body(): lax.all_to_all(packed, 'kv', split_axis=0, concat_axis=0, tiled=True)]
    unnamed x24 -> x2, local copies, waits for them, and re-layouts: 2.35 us -> 4.39 us
    add x1 -> x0, other arithmetic: 1.93 us -> none  [body(): retain[..., None] * states]
  transfers between devices with their start and end apart: 1 -> 0, of which waited for: 1 -> 0; matrix products, arithmetic and copies ran while one was open for 0% -> 0% of each run, Pallas kernels for 0% -> 0%
where the time goes in v1:
time: 48.1 us; the launch traced here: 47.9 us
  Pallas kernels  42.9 us (89%)
  local copies, waits for them, and re-layouts  4.39 us (9%)
  between operations  0.65 us (1%)
    pallas_call x1, Pallas kernels, fused(): pl.pallas_call(functools.partial(layer_kernel, groups, halves), out_shape...  42.9 us
    unnamed x2, local copies, waits for them, and re-layouts  4.39 us

profile of v1, /device:TPU:0, one launch (start us, length us, event | category | flops | bytes accessed | tf_op | source)
XLA Modules:
  0.0 47.9 jit_solution(8867467922371215894)
XLA Ops:
  0.6 42.9 %shard_map.167 = (bf16[8,512]{1,0:T(8,128)(2,1)}, f32[2,8,128,256]{3,2,1,0:T(8,128)}) custom-call(bf16[8,512]{1,0:T(8,128)(2,1)} %tokens.1, bf16[256,4096]{1,0:T(8,128)(2,1)} %bitcast.21, bf16[256,4096]{1,0:T(8,128)(2,1)} %bitcast.22, bf16[256,4096]{1,0:T(8,128)(2,1)} %bitcast.23, bf16[512,4096]{1,0:T(8,128)(2,1)} %bitcast.19, bf16[512,4096]{1,0:T(8,128)(2,1)} %bitcast.20, ...), custom_call_target="tpu_custom_call" | custom-call | tf_op jit(solution)/shard_map/pallas_call | solution.py:420
  43.5 1.3 %copy.20 = bf16[8,512]{1,0:T(8,128)(2,1)} copy(bf16[8,512]{1,0:T(8,128)(2,1)} %get-tuple-element.4) | data formatting | bytes 16384
  44.8 3.1 %copy.21 = f32[2,8,128,256]{3,2,1,0:T(8,128)} copy(f32[2,8,128,256]{3,2,1,0:T(8,128)} %get-tuple-element.5) | data formatting | bytes 4194304
